TPU v7x, 32 devices: a whole 2x2x4 slice. The times are simulated.
32 devices in a mesh: ep: 8 (over z, core), tp: 4 (over y, x).
Axes of the slice: x: 2, y: 2, z: 4, core: 2. Of those that a mesh axis runs over, the one named last changes fastest.
Arguments:
- tokens: bfloat16 [256, 4096], P('ep'), may hold values from -6 to 6
- recur_state: float32 [256, 4096], P('ep', 'tp'), may hold values from -6 to 6
- conv_state: bfloat16 [256, 3, 4096], P('ep', None, 'tp'), may hold values from -6 to 6
- mix_gain: float32 [4096], replicated, may hold values from 0.1 to 1.9
- in_weight: bfloat16 [4096, 4096], P('ep', 'tp'), may hold values from -0.09375 to 0.09375
- gate_weight: bfloat16 [4096, 4096], P('ep', 'tp'), may hold values from -0.09375 to 0.09375
- conv_taps: float32 [4, 4096], P(None, 'tp'), may hold values from -3 to 3
- recur_gate_blocks: bfloat16 [64, 64, 64], P('tp'), may hold values from -0.75 to 0.75
- input_gate_blocks: bfloat16 [64, 64, 64], P('tp'), may hold values from -0.75 to 0.75
- decay_rate: float32 [4096], P('tp'), may hold values from 0.01 to 0.4
- out_weight: bfloat16 [4096, 4096], P('tp', 'ep'), may hold values from -0.09375 to 0.09375
- ffn_gain: float32 [4096], replicated, may hold values from 0.1 to 1.9
- router_weight: bfloat16 [4096, 8], replicated, may hold values from -0.09375 to 0.09375
- routes: int32 [256, 2], P('ep'), may hold values from 0 to 7, as said below
- expert_gate: bfloat16 [8, 4096, 2048], P('ep', None, 'tp'), may hold values from -0.09375 to 0.09375
- expert_up: bfloat16 [8, 4096, 2048], P('ep', None, 'tp'), may hold values from -0.09375 to 0.09375
- expert_down: bfloat16 [8, 2048, 4096], P('ep', 'tp'), may hold values from -0.125 to 0.125
- dense_gate: bfloat16 [4096, 2048], P('ep', 'tp'), may hold values from -0.09375 to 0.09375
- dense_up: bfloat16 [4096, 2048], P('ep', 'tp'), may hold values from -0.09375 to 0.09375
- dense_down: bfloat16 [2048, 4096], P('tp', 'ep'), may hold values from -0.125 to 0.125
- branch_gate: bfloat16 [4096], replicated, may hold values from -0.09375 to 0.09375
Outputs:
- layer_out: bfloat16 [256, 4096], P('ep')
- new_state: float32 [256, 4096], P('ep', 'tp')
- new_conv_state: bfloat16 [256, 3, 4096], P('ep', None, 'tp')
Inputs may be any that keep to these rules, and one draw needn't show every extreme that they name: `routes`: A row names two different experts of one group: both have the same e // 4. In the rows of one index of ep no expert is named more than 16 times, and in every draw some expert is named exactly 16 times by the rows of every index of ep.
All inputs are finite; a program needn't handle non-finite values.
Results may differ from a plain program's by a relative error of at most 0.023.
Values may be sent and summed in bfloat16 or wider, within the bound.
A program may use at most 64 MiB of HBM per device.

v0:
```python
import jax
import jax.numpy as jnp
from jax import lax
from jax.sharding import PartitionSpec as P

TOP_K = 2
epsilon = 1e-06
decay_scale = 8.0


def rms_scale(rows, gain):
    values = rows.astype(jnp.float32)
    inverse = lax.rsqrt(jnp.mean(values * values, axis=-1, keepdims=True) + epsilon)
    return (values * inverse * gain).astype(jnp.bfloat16)


def on_device(
    tokens,
    recur_state,
    conv_state,
    mix_gain,
    in_weight,
    gate_weight,
    conv_taps,
    recur_gate_blocks,
    input_gate_blocks,
    decay_rate,
    out_weight,
    ffn_gain,
    router_weight,
    routes,
    expert_gate,
    expert_up,
    expert_down,
    dense_gate,
    dense_up,
    dense_down,
    branch_gate,
):
    batch_rows, width = tokens.shape
    channels = in_weight.shape[1]
    normed = rms_scale(tokens, mix_gain)
    arrived = lax.all_to_all(normed, "ep", split_axis=1, concat_axis=0, tiled=True)
    joined = jnp.concatenate([in_weight, gate_weight], axis=1)
    summed = lax.psum_scatter(
        jnp.dot(arrived, joined, preferred_element_type=jnp.float32).astype(jnp.bfloat16),
        "ep",
        scatter_dimension=0,
        tiled=True,
    ).astype(jnp.float32)
    x_sum, gate_sum = (summed[:, :channels], summed[:, channels:])
    x_branch = x_sum.astype(jnp.bfloat16)
    gate_branch = gate_sum.astype(jnp.bfloat16)
    window = jnp.concatenate([conv_state, x_branch[:, None, :]], axis=1)
    conv_out = jnp.sum(window.astype(jnp.float32) * conv_taps[None], axis=1).astype(jnp.bfloat16)
    new_conv_state = window[:, 1:, :]
    blocks = conv_out.reshape(batch_rows, recur_gate_blocks.shape[0], recur_gate_blocks.shape[1])
    recur_gate = jax.nn.sigmoid(
        jnp.einsum(
            "bhi,hij->bhj", blocks, recur_gate_blocks, preferred_element_type=jnp.float32
        ).reshape(batch_rows, channels)
    )
    input_gate = jax.nn.sigmoid(
        jnp.einsum(
            "bhi,hij->bhj", blocks, input_gate_blocks, preferred_element_type=jnp.float32
        ).reshape(batch_rows, channels)
    )
    log_decay = -decay_scale * recur_gate * decay_rate
    new_state = jnp.exp(log_decay) * recur_state + jnp.sqrt(
        -jnp.expm1(2.0 * log_decay)
    ) * input_gate * conv_out.astype(jnp.float32)
    mixer_rows = (new_state * jax.nn.gelu(gate_branch.astype(jnp.float32))).astype(jnp.bfloat16)
    mixer_part = jnp.dot(
        mixer_rows,
        lax.all_gather(out_weight, "ep", axis=1, tiled=True),
        preferred_element_type=jnp.float32,
    )
    resid = (
        tokens.astype(jnp.float32)
        + lax.psum(mixer_part.astype(jnp.bfloat16), "tp").astype(jnp.float32)
    ).astype(jnp.bfloat16)
    normed_ffn = rms_scale(resid, ffn_gain)
    router_logits = jnp.dot(normed_ffn, router_weight, preferred_element_type=jnp.float32)
    experts = router_logits.shape[1]
    expert_ids = lax.broadcasted_iota(jnp.int32, (batch_rows, TOP_K, experts), 2)
    picked = jnp.sum(
        jnp.where(routes[:, :, None] == expert_ids, router_logits[:, None, :], 0.0), axis=2
    )
    route_weight = jax.nn.sigmoid(picked - picked[:, ::-1]).astype(jnp.bfloat16)
    capacity = 2 * batch_rows * TOP_K // experts
    flat_ids = routes.reshape(batch_rows * TOP_K)
    onehot = (
        flat_ids[:, None] == lax.broadcasted_iota(jnp.int32, (batch_rows * TOP_K, experts), 1)
    ).astype(jnp.int32)
    rank = jnp.sum((jnp.cumsum(onehot, axis=0) - onehot) * onehot, axis=1)
    slot_of = (flat_ids * capacity + rank).reshape(batch_rows, TOP_K)
    slot_rows = lax.broadcasted_iota(jnp.int32, (experts * capacity, batch_rows), 0)
    slot_cols = lax.broadcasted_iota(jnp.int32, (batch_rows, experts * capacity), 1)
    dispatch = jnp.zeros((experts * capacity, batch_rows), jnp.bfloat16)
    combine = jnp.zeros((batch_rows, experts * capacity), jnp.bfloat16)
    for pick in range(TOP_K):
        dispatch = dispatch + (slot_rows == slot_of[None, :, pick]).astype(jnp.bfloat16)
        combine = combine + jnp.where(
            slot_cols == slot_of[:, pick : pick + 1],
            route_weight[:, pick : pick + 1],
            jnp.zeros((), jnp.bfloat16),
        )
    outgoing = (
        jnp.dot(dispatch, normed_ffn, preferred_element_type=jnp.float32)
        .astype(jnp.bfloat16)
        .reshape(experts, capacity, width)
    )
    gate_local = expert_gate[0]
    up_local = expert_up[0]
    down_local = expert_down[0]
    arrived_rows = lax.all_to_all(outgoing, "ep", split_axis=0, concat_axis=0, tiled=True)
    sources, items, features = arrived_rows.shape
    rows = arrived_rows.reshape(sources * items, features)
    first = jnp.dot(rows, gate_local, preferred_element_type=jnp.float32)
    second = jnp.dot(rows, up_local, preferred_element_type=jnp.float32)
    act = (jax.nn.silu(first) * second).astype(jnp.bfloat16)
    partial_value = jnp.dot(act, down_local, preferred_element_type=jnp.float32)
    total = lax.psum(partial_value.astype(jnp.bfloat16), "tp")
    returned = lax.all_to_all(
        total.reshape(sources, items, total.shape[1]), "ep", split_axis=0, concat_axis=0, tiled=True
    )
    moe = jnp.dot(
        combine,
        returned.reshape(experts * capacity, returned.shape[2]),
        preferred_element_type=jnp.float32,
    )
    dense_arrived = lax.all_to_all(normed_ffn, "ep", split_axis=1, concat_axis=0, tiled=True)
    dense_joined = jnp.concatenate([dense_gate, dense_up], axis=1)
    dense_summed = lax.psum_scatter(
        jnp.dot(dense_arrived, dense_joined, preferred_element_type=jnp.float32).astype(
            jnp.bfloat16
        ),
        "ep",
        scatter_dimension=0,
        tiled=True,
    ).astype(jnp.float32)
    dense_first = dense_summed[:, : dense_gate.shape[1]]
    dense_second = dense_summed[:, dense_gate.shape[1] :]
    dense_act = (jax.nn.silu(dense_first) * dense_second).astype(jnp.bfloat16)
    dense_part = jnp.dot(
        dense_act,
        lax.all_gather(dense_down, "ep", axis=1, tiled=True),
        preferred_element_type=jnp.float32,
    )
    branch_weight = jax.nn.sigmoid(
        jnp.dot(normed_ffn, branch_gate, preferred_element_type=jnp.float32)
    )
    dense_sum = lax.psum(dense_part.astype(jnp.bfloat16), "tp").astype(jnp.float32)
    layer_out = (resid.astype(jnp.float32) + moe + branch_weight[:, None] * dense_sum).astype(
        jnp.bfloat16
    )
    return (layer_out, new_state, new_conv_state)


def solution(mesh):
    in_specs = (
        P("ep", None),
        P("ep", "tp"),
        P("ep", None, "tp"),
        P(),
        P("ep", "tp"),
        P("ep", "tp"),
        P(None, "tp"),
        P("tp", None, None),
        P("tp", None, None),
        P("tp"),
        P("tp", "ep"),
        P(),
        P(),
        P("ep", None),
        P("ep", None, "tp"),
        P("ep", None, "tp"),
        P("ep", "tp", None),
        P("ep", "tp"),
        P("ep", "tp"),
        P("tp", "ep"),
        P(),
    )
    out_specs = (P("ep", None), P("ep", "tp"), P("ep", None, "tp"))
    return jax.shard_map(
        on_device, mesh=mesh, in_specs=in_specs, out_specs=out_specs, check_vma=False
    )
```

profile of v0, /device:TPU:0, one launch (start us, length us, event | category | flops | bytes accessed | tf_op | source)
XLA Modules:
  0.0 396.9 jit_solution(11186199223250125864)
XLA Ops:
  7.2 1.1 fusion.33
  8.4 1.1 fusion.35
  9.5 16.0 %all_to_all.48 = bf16[32,8,512]{2,0,1:T(8,128)(2,1)S(1)} all-to-all(bf16[32,8,512]{2,0,1:T(8,128)(2,1)S(1)} %bitcast.77), channel_id=1, replica_groups=mesh['ep'=8,'tp'=4] {'ep'}, dimensions={1} | all-to-all | bytes 524288 | tf_op jit(solution)/shard_map/all_to_all | solution.py:43
  25.5 3.4 convolution_convert_fusion.4
  29.0 0.7 all-gather.3.cloned.1.call-update
  29.8 30.9 %reduce-scatter.3.cloned.1.call-done = bf16[32,2048]{1,0:T(8,128)(2,1)} async-done(((bf16[256,2048]{1,0:T(8,128)(2,1)}), bf16[32,2048]{1,0:T(8,128)(2,1)}) %reduce-scatter.3.cloned.1.call-update) | async-done | bytes 131088 | tf_op jit(solution)/shard_map/reduce_scatter | solution.py:45
  60.7 0.9 slice_bitcast_fusion
  61.9 0.2 fusion.17
  62.4 0.2 fusion.13
  63.1 79.5 %all-gather.3.cloned.1.call-done = bf16[1024,4096]{1,0:T(8,128)(2,1)} async-done(((bf16[1024,512]{1,0:T(8,128)(2,1)}), bf16[1024,4096]{1,0:T(8,128)(2,1)}) %all-gather.3.cloned.1.call-update) | async-done | bytes 8388624 | tf_op jit(solution)/shard_map/all_gather | solution.py:75
  142.5 5.6 %convolution_convert_fusion.3 = bf16[32,4096]{1,0:T(8,128)(2,1)} fusion(bf16[1024,4096]{1,0:T(8,128)(2,1)} %all-gather.3.cloned.1.call-done, f32[32,1024]{1,0:T(8,128)S(1)} %multiply_add_fusion, bf16[32,2048]{1,0:T(8,128)(2,1)S(1)} %copy-done.5), kind=kOutput, calls=%fused_computation.6 | convolution fusion | flops 268926976 | bytes 8847360 | tf_op jit(solution)/shard_map/dot_general | solution.py:73
  148.2 41.6 %all-reduce.4.cloned.1.call-done = bf16[32,4096]{1,0:T(8,128)(2,1)} async-done(((bf16[32,4096]{1,0:T(8,128)(2,1)}), bf16[32,4096]{1,0:T(8,128)(2,1)}) %all-reduce.4.cloned.1.call-update) | async-done | bytes 262160 | tf_op jit(solution)/shard_map/psum | solution.py:80
  189.9 1.1 fusion.37
  191.0 1.1 fusion.39
  192.1 14.1 %all_to_all.49 = bf16[32,8,512]{2,0,1:T(8,128)(2,1)S(1)} all-to-all(bf16[32,8,512]{2,0,1:T(8,128)(2,1)S(1)} %bitcast.78), channel_id=1, replica_groups=mesh['ep'=8,'tp'=4] {'ep'}, dimensions={1} | all-to-all | bytes 524288 | tf_op jit(solution)/shard_map/all_to_all | solution.py:132
  206.2 1.3 convolution_convert_fusion.5
  207.6 0.5 all-gather.5.cloned.1.call-update
  208.5 0.2 select_reduce_fusion
  208.9 1.4 convolution_convert_fusion.1
  210.3 3.6 all-to-all-start.1
  213.9 24.5 %reduce-scatter.5.cloned.1.call-done = bf16[32,1024]{1,0:T(8,128)(2,1)} async-done(((bf16[256,1024]{1,0:T(8,128)(2,1)}), bf16[32,1024]{1,0:T(8,128)(2,1)}) %reduce-scatter.5.cloned.1.call-update) | async-done | bytes 65552 | tf_op jit(solution)/shard_map/reduce_scatter | solution.py:134
  238.4 0.8 convert_element_type.109
  239.2 49.8 %all-gather.5.cloned.1.call-done = bf16[512,4096]{1,0:T(8,128)(2,1)} async-done(((bf16[512,512]{1,0:T(8,128)(2,1)}), bf16[512,4096]{1,0:T(8,128)(2,1)}) %all-gather.5.cloned.1.call-update) | async-done | bytes 4194320 | tf_op jit(solution)/shard_map/all_gather | solution.py:147
  289.0 3.7 convolution_convert_fusion.2
  292.7 2.9 fusion.5
  295.7 5.9 %convolution_convert_fusion = bf16[128,4096]{1,0:T(8,128)(2,1)} fusion(bf16[1,512,4096]{2,1,0:T(8,128)(2,1)} %param.37, bf16[128,4096]{1,0:T(8,128)(2,1)S(1)} %bitcast.72, bf16[1,4096,512]{2,1,0:T(8,128)(2,1)} %param.36, f32[128,512]{1,0:T(8,128)S(1)} %fusion.5), kind=kOutput, calls=%fused_computation | convolution fusion | flops 1074659328 | bytes 10747904 | tf_op jit(solution)/shard_map/dot_general | solution.py:122
  301.6 55.4 %all-reduce.6.cloned.1.call-done = (bf16[8,16,4096]{2,1,0:T(8,128)(2,1)}, bf16[32,4096]{1,0:T(8,128)(2,1)}) async-done(((bf16[8,16,4096]{2,1,0:T(8,128)(2,1)}, bf16[32,4096]{1,0:T(8,128)(2,1)}), (bf16[8,16,4096]{2,1,0:T(8,128)(2,1)}, bf16[32,4096]{1,0:T(8,128)(2,1)})) %all-reduce.6.cloned.1.call-update) | async-done | bytes 1310736 | tf_op jit(solution)/shard_map/psum | solution.py:123
  356.9 4.6 %all-to-all-start.2 = ((bf16[8,16,4096]{2,1,0:T(8,128)(2,1)}), bf16[8,16,4096]{2,1,0:T(8,128)(2,1)S(1)}, u32[]{:S(2)}, u32[]{:S(2)}) async-start(bf16[8,16,4096]{2,1,0:T(8,128)(2,1)} %get-tuple-element.3), calls=%async_computation.3 | async-start | bytes 2097152 | tf_op jit(solution)/shard_map/all_to_all | solution.py:124
  361.5 0.7 fusion.45
  362.5 0.2 fusion.27
  362.7 25.4 %all-to-all-done.2 = bf16[8,16,4096]{2,1,0:T(8,128)(2,1)S(1)} async-done(((bf16[8,16,4096]{2,1,0:T(8,128)(2,1)}), bf16[8,16,4096]{2,1,0:T(8,128)(2,1)S(1)}, u32[]{:S(2)}, u32[]{:S(2)}) %all-to-all-start.2) | async-done | bytes 1048608 | tf_op jit(solution)/shard_map/all_to_all | solution.py:124
  388.1 2.0 fusion.1
  (69 shorter events, 2.2 us)
Async XLA Ops:
  7.2 54.7 %copy-start = (bf16[16,64,64]{2,1,0:T(8,128)(2,1)S(1)}, bf16[16,64,64]{2,1,0:T(8,128)(2,1)}, u32[]{:S(2)}) copy-start(bf16[16,64,64]{2,1,0:T(8,128)(2,1)} %param.28) | copy-start | bytes 393220
  7.2 53.5 %reduce-scatter.3.cloned.1.call-start = ((), (), s32[]{:S(2)}) async-start(), calls=%async_computation.6 | async-start | bytes 1179648 | tf_op jit(solution)/shard_map/reduce_scatter | solution.py:45
  8.4 21.4 %copy-start.12 = (f32[1024]{0:T(1024)S(1)}, f32[1024]{0:T(1024)}, u32[]{:S(2)}) copy-start(f32[1024]{0:T(1024)} %param.30) | copy-start | bytes 12292
  9.5 52.1 %copy-start.4 = (bf16[32,3,1024]{2,0,1:T(8,128)(2,1)S(1)}, bf16[32,3,1024]{2,0,1:T(8,128)(2,1)}, u32[]{:S(2)}) copy-start(bf16[32,3,1024]{2,0,1:T(8,128)(2,1)} %param.23) | copy-start | bytes 589828
  9.5 52.1 %copy-start.9 = (f32[4,1024]{1,0:T(4,128)S(1)}, f32[4,1024]{1,0:T(4,128)}, u32[]{:S(2)}) copy-start(f32[4,1024]{1,0:T(4,128)} %param.27) | copy-start | bytes 49156
  25.5 36.8 %copy-start.15 = (bf16[16,64,64]{2,1,0:T(8,128)(2,1)S(1)}, bf16[16,64,64]{2,1,0:T(8,128)(2,1)}, u32[]{:S(2)}) copy-start(bf16[16,64,64]{2,1,0:T(8,128)(2,1)} %param.29) | copy-start | bytes 393220
  28.9 34.0 %copy-start.6 = (f32[32,1024]{1,0:T(8,128)S(1)}, f32[32,1024]{1,0:T(8,128)}, u32[]{:S(2)}) copy-start(f32[32,1024]{1,0:T(8,128)} %param.22) | copy-start | bytes 393220
  28.9 113.6 %all-gather.3.cloned.1.call-start = ((), (), s32[]{:S(2)}) async-start(), calls=%async_computation.7 | async-start | bytes 9437184 | tf_op jit(solution)/shard_map/all_gather | solution.py:75
  29.7 160.2 %all-reduce.4.cloned.1.call-start = ((), (), s32[]{:S(2)}) async-start(), calls=%async_computation.8 | async-start | bytes 524288 | tf_op jit(solution)/shard_map/psum | solution.py:80
  60.7 81.8 %copy-start.5 = (bf16[32,2048]{1,0:T(8,128)(2,1)S(1)}, bf16[32,2048]{1,0:T(8,128)(2,1)}, u32[]{:S(2)}) copy-start(bf16[32,2048]{1,0:T(8,128)(2,1)} %reduce-scatter.3.cloned.1.call-done) | copy-start | bytes 393220
  63.0 85.1 %copy-start.3 = (f32[32,1024]{1,0:T(8,128)}, f32[32,1024]{1,0:T(8,128)S(1)}, u32[]{:S(2)}) copy-start(f32[32,1024]{1,0:T(8,128)S(1)} %multiply_add_fusion) | copy-start | bytes 393220
  63.0 126.8 %copy-start.1 = (bf16[32,4096]{1,0:T(8,128)(2,1)S(1)}, bf16[32,4096]{1,0:T(8,128)(2,1)}, u32[]{:S(2)}) copy-start(bf16[32,4096]{1,0:T(8,128)(2,1)} %param.21) | copy-start | bytes 786436
  63.0 128.0 %copy-start.8 = (f32[4096]{0:T(1024)S(1)}, f32[4096]{0:T(1024)}, u32[]{:S(2)}) copy-start(f32[4096]{0:T(1024)} %param.32) | copy-start | bytes 49156
  63.1 143.2 %copy-start.13 = (bf16[512,512]{1,0:T(8,128)(2,1)S(1)}, bf16[512,512]{1,0:T(8,128)(2,1)}, u32[]{:S(2)}) copy-start(bf16[512,512]{1,0:T(8,128)(2,1)} %param.39) | copy-start | bytes 1572868
  63.1 143.2 %copy-start.14 = (bf16[512,512]{1,0:T(8,128)(2,1)S(1)}, bf16[512,512]{1,0:T(8,128)(2,1)}, u32[]{:S(2)}) copy-start(bf16[512,512]{1,0:T(8,128)(2,1)} %param.38) | copy-start | bytes 1572868
  148.2 60.0 %copy-start.10 = (s32[32,2]{0,1:T(2,128)S(1)}, s32[32,2]{0,1:T(2,128)}, u32[]{:S(2)}) copy-start(s32[32,2]{0,1:T(2,128)} %param.34) | copy-start | bytes 772
  148.2 90.2 %reduce-scatter.5.cloned.1.call-start = ((), (), s32[]{:S(2)}) async-start(), calls=%async_computation.9 | async-start | bytes 589824 | tf_op jit(solution)/shard_map/reduce_scatter | solution.py:134
  207.6 81.4 %all-gather.5.cloned.1.call-start = ((), (), s32[]{:S(2)}) async-start(), calls=%async_computation.10 | async-start | bytes 4718592 | tf_op jit(solution)/shard_map/all_gather | solution.py:147
  210.3 82.4 %all-to-all-start.1 = ((bf16[8,16,4096]{2,1,0:T(8,128)(2,1)}), bf16[8,16,4096]{2,1,0:T(8,128)(2,1)S(1)}, u32[]{:S(2)}, u32[]{:S(2)}) async-start(bf16[8,16,4096]{2,1,0:T(8,128)(2,1)} %bitcast.9), calls=%async_computation.2 | async-start | bytes 2097152 | tf_op jit(solution)/shard_map/all_to_all | solution.py:116
  213.9 143.0 %all-reduce.6.cloned.1.call-start = ((), (), s32[]{:S(2)}) async-start(), calls=%async_computation.11 | async-start | bytes 2621440 | tf_op jit(solution)/shard_map/psum | solution.py:123
  295.6 65.9 %copy-start.11 = (bf16[4096]{0:T(1024)(128)(2,1)S(1)}, bf16[4096]{0:T(1024)(128)(2,1)}, u32[]{:S(2)}) copy-start(bf16[4096]{0:T(1024)(128)(2,1)} %param.41) | copy-start | bytes 24580
  295.6 66.6 %copy-start.7 = (bf16[4096,8]{0,1:T(8,128)(2,1)S(1)}, bf16[4096,8]{0,1:T(8,128)(2,1)}, u32[]{:S(2)}) copy-start(bf16[4096,8]{0,1:T(8,128)(2,1)} %param.33) | copy-start | bytes 196612
  301.5 86.5 %copy-start.2 = (bf16[32,4096]{1,0:T(8,128)(2,1)S(1)}, bf16[32,4096]{1,0:T(8,128)(2,1)}, u32[]{:S(2)}) copy-start(bf16[32,4096]{1,0:T(8,128)(2,1)} %all-reduce.4.cloned.1.call-done) | copy-start | bytes 786436
  356.9 31.2 %all-to-all-start.2 = ((bf16[8,16,4096]{2,1,0:T(8,128)(2,1)}), bf16[8,16,4096]{2,1,0:T(8,128)(2,1)S(1)}, u32[]{:S(2)}, u32[]{:S(2)}) async-start(bf16[8,16,4096]{2,1,0:T(8,128)(2,1)} %get-tuple-element.3), calls=%async_computation.3 | async-start | bytes 2097152 | tf_op jit(solution)/shard_map/all_to_all | solution.py:124
Sparse Core Ops, SparseCore 0:
  29.1 31.6 reduce-scatter.2
  62.3 80.1 all-gather.2
  148.3 41.5 all-reduce.3
  207.7 30.6 reduce-scatter.4
  239.8 49.1 all-gather.4
  301.7 55.1 all-reduce.5
where the time goes:
time: 398 us; the launch traced here: 397 us
  waiting for transfers between devices  308 us (77%)
  blocking collectives  30.1 us (8%)
  matrix products  26.9 us (7%)
  between operations  14.4 us (4%)
  starting transfers between devices  8.4 us (2%)
  other arithmetic  6.59 us (2%)
    all_gather x1, waiting for transfers between devices, on_device(): lax.all_gather(out_weight, 'ep', axis=1, tiled=True)  79.5 us
    psum x1, waiting for transfers between devices, on_device(): total = lax.psum(partial_value.astype(jnp.bfloat16), 'tp')  55.4 us
    all_gather x1, waiting for transfers between devices, on_device(): lax.all_gather(dense_down, 'ep', axis=1, tiled=True)  49.8 us
    psum x1, waiting for transfers between devices, on_device(): lax.psum(mixer_part.astype(jnp.bfloat16), 'tp').astype(jnp.float32)  41.6 us
    reduce_scatter x1, waiting for transfers between devices, on_device(): lax.psum_scatter(jnp.dot(arrived, joined, preferred_element_type=jnp.floa...  30.9 us
    all_to_all x1, waiting for transfers between devices, on_device(): lax.all_to_all(total.reshape(sources, items, total.shape[1]), 'ep', split...  25.4 us
    reduce_scatter x1, waiting for transfers between devices, on_device(): lax.psum_scatter(jnp.dot(dense_arrived, dense_joined, preferred_element_t...  24.5 us
    all_to_all x1, blocking collectives, on_device(): lax.all_to_all(normed, 'ep', split_axis=1, concat_axis=0, tiled=True)  16 us
  transfers between devices with their start and end apart: 8, of which 7 were waited for; matrix products, arithmetic and copies ran while one was open for 3% of the time, Pallas kernels for 0%

commit v1 on v0

--- a/solution.py
+++ b/solution.py
@@ -72,7 +72,9 @@
     mixer_rows = (new_state * jax.nn.gelu(gate_branch.astype(jnp.float32))).astype(jnp.bfloat16)
     mixer_part = jnp.dot(
         mixer_rows,
-        lax.all_gather(out_weight, "ep", axis=1, tiled=True),
+        jnp.concatenate(
+            lax.all_to_all(jnp.stack([out_weight] * lax.axis_size("ep")), "ep", 0, 0), axis=1
+        ),
         preferred_element_type=jnp.float32,
     )
     resid = (

time: 398 us -> 486 us (1.22)
  waiting for transfers between devices: 308 us -> 394 us
  blocking collectives: 30.1 us -> 14.1 us
  starting transfers between devices: 8.4 us -> 19.8 us
  local copies, waits for them, and re-layouts: 2.18 us -> 8.69 us
    all_to_all x0 -> x2, waiting for transfers between devices: none -> 146 us  [the longest x1 138 us: on_device(): lax.all_to_all(jnp.stack([out_weight] * lax.axis_size('ep')), 'ep', 0, 0)]
    all_gather x1 -> x0, waiting for transfers between devices: 79.5 us -> none  [on_device(): lax.all_gather(out_weight, 'ep', axis=1, tiled=True)]
    reduce_scatter x1, waiting for transfers between devices: 30.9 us -> 50.9 us  [on_device(): lax.psum_scatter(jnp.dot(arrived, joined, preferred_element_type=jnp.floa...]
    all_to_all x1 -> x0, blocking collectives: 16 us -> none  [on_device(): lax.all_to_all(normed, 'ep', split_axis=1, concat_axis=0, tiled=True)]
    all_to_all x0 -> x2, starting transfers between devices: none -> 11.4 us  [the longest x1 6.35 us: on_device(): lax.all_to_all(normed, 'ep', split_axis=1, concat_axis=0, tiled=True)]
  transfers between devices with their start and end apart: 8 -> 9, of which waited for: 7 -> 8; matrix products, arithmetic and copies ran while one was open for 3% -> 3% of each run, Pallas kernels for 0% -> 0%
where the time goes in v1:
time: 486 us; the launch traced here: 485 us
  waiting for transfers between devices  394 us (81%)
  matrix products  27.3 us (6%)
  starting transfers between devices  19.8 us (4%)
  blocking collectives  14.1 us (3%)
  between operations  14.1 us (3%)
  local copies, waits for them, and re-layouts  8.69 us (2%)
  other arithmetic  6.6 us (1%)
    all_to_all x1, waiting for transfers between devices, on_device(): lax.all_to_all(jnp.stack([out_weight] * lax.axis_size('ep')), 'ep', 0, 0)  138 us
    psum x1, waiting for transfers between devices, on_device(): total = lax.psum(partial_value.astype(jnp.bfloat16), 'tp')  55.4 us
    reduce_scatter x1, waiting for transfers between devices, on_device(): lax.psum_scatter(jnp.dot(arrived, joined, preferred_element_type=jnp.floa...  50.9 us
    all_gather x1, waiting for transfers between devices, on_device(): lax.all_gather(dense_down, 'ep', axis=1, tiled=True)  49.7 us
    psum x1, waiting for transfers between devices, on_device(): lax.psum(mixer_part.astype(jnp.bfloat16), 'tp').astype(jnp.float32)  42.1 us
    all_to_all x1, waiting for transfers between devices, on_device(): lax.all_to_all(total.reshape(sources, items, total.shape[1]), 'ep', split...  25.4 us
    reduce_scatter x1, waiting for transfers between devices, on_device(): lax.psum_scatter(jnp.dot(dense_arrived, dense_joined, preferred_element_t...  24.5 us
    all_to_all x1, blocking collectives, on_device(): lax.all_to_all(normed_ffn, 'ep', split_axis=1, concat_axis=0, tiled=True)  14.1 us
  transfers between devices with their start and end apart: 9, of which 8 were waited for; matrix products, arithmetic and copies ran while one was open for 3% of the time, Pallas kernels for 0%

profile of v1, /device:TPU:0, one launch (start us, length us, event | category | flops | bytes accessed | tf_op | source)
XLA Modules:
  0.0 485.0 jit_solution(17756099059100083999)
XLA Ops:
  7.2 1.2 fusion.33
  8.3 1.1 fusion.35
  9.4 0.7 copy.73
  10.2 6.4 %all-to-all-start = ((bf16[32,8,512]{2,0,1:T(8,128)(2,1)}), bf16[32,8,512]{2,0,1:T(8,128)(2,1)S(1)}, u32[]{:S(2)}, u32[]{:S(2)}) async-start(bf16[32,8,512]{2,0,1:T(8,128)(2,1)} %bitcast.73), calls=%async_computation | async-start | bytes 524288 | tf_op jit(solution)/shard_map/all_to_all | solution.py:43
  16.5 1.5 copy.60
  18.0 8.2 %all-to-all-done = bf16[32,8,512]{2,0,1:T(8,128)(2,1)S(1)} async-done(((bf16[32,8,512]{2,0,1:T(8,128)(2,1)}), bf16[32,8,512]{2,0,1:T(8,128)(2,1)S(1)}, u32[]{:S(2)}, u32[]{:S(2)}) %all-to-all-start) | async-done | bytes 262176 | tf_op jit(solution)/shard_map/all_to_all | solution.py:43
  26.2 4.3 stack.2
  30.6 5.1 %all-to-all-start.1 = ((bf16[8,1024,512]{1,2,0:T(8,128)(2,1)}), bf16[8,1024,512]{1,2,0:T(8,128)(2,1)}, u32[]{:S(2)}, u32[]{:S(2)}) async-start(bf16[8,1024,512]{1,2,0:T(8,128)(2,1)} %stack.2), calls=%async_computation.2 | async-start | bytes 16777216 | tf_op jit(solution)/shard_map/all_to_all | solution.py:76
  35.8 1.7 convolution_convert_fusion.4
  37.6 50.9 %reduce-scatter.3.cloned.1.call-done = bf16[32,2048]{1,0:T(8,128)(2,1)} async-done(((bf16[256,2048]{1,0:T(8,128)(2,1)}), bf16[32,2048]{1,0:T(8,128)(2,1)}) %reduce-scatter.3.cloned.1.call-update) | async-done | bytes 131088 | tf_op jit(solution)/shard_map/reduce_scatter | solution.py:45
  88.4 0.9 slice_bitcast_fusion
  90.1 1.2 fusion.17
  91.7 137.7 %all-to-all-done.1 = bf16[8,1024,512]{1,2,0:T(8,128)(2,1)} async-done(((bf16[8,1024,512]{1,2,0:T(8,128)(2,1)}), bf16[8,1024,512]{1,2,0:T(8,128)(2,1)}, u32[]{:S(2)}, u32[]{:S(2)}) %all-to-all-start.1) | async-done | bytes 8388640 | tf_op jit(solution)/shard_map/all_to_all | solution.py:76
  229.4 6.7 %convolution_convert_fusion.3 = bf16[32,4096]{1,0:T(8,128)(2,1)} fusion(bf16[1024,4096]{0,1:T(8,128)(2,1)} %bitcast.6, f32[32,1024]{1,0:T(8,128)S(1)} %multiply_add_fusion, bf16[32,2048]{1,0:T(8,128)(2,1)S(1)} %copy-done.5), kind=kOutput, calls=%fused_computation.6 | convolution fusion | flops 268926976 | bytes 8847360 | tf_op jit(solution)/shard_map/dot_general | solution.py:73
  236.2 42.1 %all-reduce.4.cloned.1.call-done = bf16[32,4096]{1,0:T(8,128)(2,1)} async-done(((bf16[32,4096]{1,0:T(8,128)(2,1)}), bf16[32,4096]{1,0:T(8,128)(2,1)}) %all-reduce.4.cloned.1.call-update) | async-done | bytes 262160 | tf_op jit(solution)/shard_map/psum | solution.py:82
  278.3 1.1 fusion.37
  279.4 1.1 fusion.39
  280.5 14.1 %all_to_all.53 = bf16[32,8,512]{2,0,1:T(8,128)(2,1)S(1)} all-to-all(bf16[32,8,512]{2,0,1:T(8,128)(2,1)S(1)} %bitcast.80), channel_id=1, replica_groups=mesh['ep'=8,'tp'=4] {'ep'}, dimensions={1} | all-to-all | bytes 524288 | tf_op jit(solution)/shard_map/all_to_all | solution.py:134
  294.6 1.3 convolution_convert_fusion.5
  297.3 1.4 convolution_convert_fusion.1
  298.7 3.6 all-to-all-start.2
  302.3 24.5 %reduce-scatter.5.cloned.1.call-done = bf16[32,1024]{1,0:T(8,128)(2,1)} async-done(((bf16[256,1024]{1,0:T(8,128)(2,1)}), bf16[32,1024]{1,0:T(8,128)(2,1)}) %reduce-scatter.5.cloned.1.call-update) | async-done | bytes 65552 | tf_op jit(solution)/shard_map/reduce_scatter | solution.py:136
  326.8 0.8 convert_element_type.109
  327.6 49.7 %all-gather.2.cloned.1.call-done = bf16[512,4096]{1,0:T(8,128)(2,1)} async-done(((bf16[512,512]{1,0:T(8,128)(2,1)}), bf16[512,4096]{1,0:T(8,128)(2,1)}) %all-gather.2.cloned.1.call-update) | async-done | bytes 4194320 | tf_op jit(solution)/shard_map/all_gather | solution.py:149
  377.4 3.7 convolution_convert_fusion.2
  381.1 2.9 fusion.5
  384.0 5.9 %convolution_convert_fusion = bf16[128,4096]{1,0:T(8,128)(2,1)} fusion(bf16[1,512,4096]{2,1,0:T(8,128)(2,1)} %param.37, bf16[128,4096]{1,0:T(8,128)(2,1)S(1)} %bitcast.75, bf16[1,4096,512]{2,1,0:T(8,128)(2,1)} %param.36, f32[128,512]{1,0:T(8,128)S(1)} %fusion.5), kind=kOutput, calls=%fused_computation | convolution fusion | flops 1074659328 | bytes 10747904 | tf_op jit(solution)/shard_map/dot_general | solution.py:124
  389.9 55.4 %all-reduce.6.cloned.1.call-done = (bf16[8,16,4096]{2,1,0:T(8,128)(2,1)}, bf16[32,4096]{1,0:T(8,128)(2,1)}) async-done(((bf16[8,16,4096]{2,1,0:T(8,128)(2,1)}, bf16[32,4096]{1,0:T(8,128)(2,1)}), (bf16[8,16,4096]{2,1,0:T(8,128)(2,1)}, bf16[32,4096]{1,0:T(8,128)(2,1)})) %all-reduce.6.cloned.1.call-update) | async-done | bytes 1310736 | tf_op jit(solution)/shard_map/psum | solution.py:125
  445.3 4.6 all-to-all-start.3
  449.9 0.7 fusion.45
  451.0 25.4 %all-to-all-done.3 = bf16[8,16,4096]{2,1,0:T(8,128)(2,1)S(1)} async-done(((bf16[8,16,4096]{2,1,0:T(8,128)(2,1)}), bf16[8,16,4096]{2,1,0:T(8,128)(2,1)S(1)}, u32[]{:S(2)}, u32[]{:S(2)}) %all-to-all-start.3) | async-done | bytes 1048608 | tf_op jit(solution)/shard_map/all_to_all | solution.py:126
  476.4 2.0 fusion.1
  (73 shorter events, 3.2 us)
Async XLA Ops:
  7.2 82.4 %copy-start = (bf16[16,64,64]{2,1,0:T(8,128)(2,1)S(1)}, bf16[16,64,64]{2,1,0:T(8,128)(2,1)}, u32[]{:S(2)}) copy-start(bf16[16,64,64]{2,1,0:T(8,128)(2,1)} %param.29) | copy-start | bytes 393220
  10.2 16.1 %all-to-all-start = ((bf16[32,8,512]{2,0,1:T(8,128)(2,1)}), bf16[32,8,512]{2,0,1:T(8,128)(2,1)S(1)}, u32[]{:S(2)}, u32[]{:S(2)}) async-start(bf16[32,8,512]{2,0,1:T(8,128)(2,1)} %bitcast.73), calls=%async_computation | async-start | bytes 524288 | tf_op jit(solution)/shard_map/all_to_all | solution.py:43
  30.6 5.2 %copy-start.13 = (bf16[512,1024]{1,0:T(8,128)(2,1)S(1)}, bf16[512,1024]{1,0:T(8,128)(2,1)}, u32[]{:S(2)}) copy-start(bf16[512,1024]{1,0:T(8,128)(2,1)} %param.26) | copy-start | bytes 3145732
  30.6 5.2 %copy-start.14 = (bf16[512,1024]{1,0:T(8,128)(2,1)S(1)}, bf16[512,1024]{1,0:T(8,128)(2,1)}, u32[]{:S(2)}) copy-start(bf16[512,1024]{1,0:T(8,128)(2,1)} %param.25) | copy-start | bytes 3145732
  30.6 198.8 %all-to-all-start.1 = ((bf16[8,1024,512]{1,2,0:T(8,128)(2,1)}), bf16[8,1024,512]{1,2,0:T(8,128)(2,1)}, u32[]{:S(2)}, u32[]{:S(2)}) async-start(bf16[8,1024,512]{1,2,0:T(8,128)(2,1)} %stack.2), calls=%async_computation.2 | async-start | bytes 16777216 | tf_op jit(solution)/shard_map/all_to_all | solution.py:76
  35.6 1.9 copy-start.12
  35.7 53.7 %copy-start.3 = (bf16[32,3,1024]{2,0,1:T(8,128)(2,1)S(1)}, bf16[32,3,1024]{2,0,1:T(8,128)(2,1)}, u32[]{:S(2)}) copy-start(bf16[32,3,1024]{2,0,1:T(8,128)(2,1)} %param.23) | copy-start | bytes 589828
  35.7 53.7 %copy-start.9 = (f32[4,1024]{1,0:T(4,128)S(1)}, f32[4,1024]{1,0:T(4,128)}, u32[]{:S(2)}) copy-start(f32[4,1024]{1,0:T(4,128)} %param.27) | copy-start | bytes 49156
  35.7 52.7 %reduce-scatter.3.cloned.1.call-start = ((), (), s32[]{:S(2)}) async-start(), calls=%async_computation.7 | async-start | bytes 1179648 | tf_op jit(solution)/shard_map/reduce_scatter | solution.py:45
  37.5 54.1 %copy-start.6 = (f32[32,1024]{1,0:T(8,128)S(1)}, f32[32,1024]{1,0:T(8,128)}, u32[]{:S(2)}) copy-start(f32[32,1024]{1,0:T(8,128)} %param.22) | copy-start | bytes 393220
  37.5 240.8 %all-reduce.4.cloned.1.call-start = ((), (), s32[]{:S(2)}) async-start(), calls=%async_computation.8 | async-start | bytes 524288 | tf_op jit(solution)/shard_map/psum | solution.py:82
  88.4 140.9 %copy-start.5 = (bf16[32,2048]{1,0:T(8,128)(2,1)S(1)}, bf16[32,2048]{1,0:T(8,128)(2,1)}, u32[]{:S(2)}) copy-start(bf16[32,2048]{1,0:T(8,128)(2,1)} %reduce-scatter.3.cloned.1.call-done) | copy-start | bytes 393220
  91.7 144.5 %copy-start.4 = (f32[32,1024]{1,0:T(8,128)}, f32[32,1024]{1,0:T(8,128)S(1)}, u32[]{:S(2)}) copy-start(f32[32,1024]{1,0:T(8,128)S(1)} %multiply_add_fusion) | copy-start | bytes 393220
  229.3 48.9 %copy-start.1 = (bf16[32,4096]{1,0:T(8,128)(2,1)S(1)}, bf16[32,4096]{1,0:T(8,128)(2,1)}, u32[]{:S(2)}) copy-start(bf16[32,4096]{1,0:T(8,128)(2,1)} %param.21) | copy-start | bytes 786436
  229.3 50.1 %copy-start.8 = (f32[4096]{0:T(1024)S(1)}, f32[4096]{0:T(1024)}, u32[]{:S(2)}) copy-start(f32[4096]{0:T(1024)} %param.32) | copy-start | bytes 49156
  229.3 65.3 %copy-start.15 = (bf16[512,512]{1,0:T(8,128)(2,1)S(1)}, bf16[512,512]{1,0:T(8,128)(2,1)}, u32[]{:S(2)}) copy-start(bf16[512,512]{1,0:T(8,128)(2,1)} %param.39) | copy-start | bytes 1572868
  229.4 65.3 %copy-start.16 = (bf16[512,512]{1,0:T(8,128)(2,1)S(1)}, bf16[512,512]{1,0:T(8,128)(2,1)}, u32[]{:S(2)}) copy-start(bf16[512,512]{1,0:T(8,128)(2,1)} %param.38) | copy-start | bytes 1572868
  236.1 60.4 %copy-start.10 = (s32[32,2]{0,1:T(2,128)S(1)}, s32[32,2]{0,1:T(2,128)}, u32[]{:S(2)}) copy-start(s32[32,2]{0,1:T(2,128)} %param.34) | copy-start | bytes 772
  236.1 90.6 %reduce-scatter.5.cloned.1.call-start = ((), (), s32[]{:S(2)}) async-start(), calls=%async_computation.9 | async-start | bytes 589824 | tf_op jit(solution)/shard_map/reduce_scatter | solution.py:136
  295.9 81.4 %all-gather.2.cloned.1.call-start = ((), (), s32[]{:S(2)}) async-start(), calls=%async_computation.10 | async-start | bytes 4718592 | tf_op jit(solution)/shard_map/all_gather | solution.py:149
  298.7 82.4 %all-to-all-start.2 = ((bf16[8,16,4096]{2,1,0:T(8,128)(2,1)}), bf16[8,16,4096]{2,1,0:T(8,128)(2,1)S(1)}, u32[]{:S(2)}, u32[]{:S(2)}) async-start(bf16[8,16,4096]{2,1,0:T(8,128)(2,1)} %bitcast.11), calls=%async_computation.3 | async-start | bytes 2097152 | tf_op jit(solution)/shard_map/all_to_all | solution.py:118
  302.3 143.0 %all-reduce.6.cloned.1.call-start = ((), (), s32[]{:S(2)}) async-start(), calls=%async_computation.11 | async-start | bytes 2621440 | tf_op jit(solution)/shard_map/psum | solution.py:125
  384.0 65.9 %copy-start.11 = (bf16[4096]{0:T(1024)(128)(2,1)S(1)}, bf16[4096]{0:T(1024)(128)(2,1)}, u32[]{:S(2)}) copy-start(bf16[4096]{0:T(1024)(128)(2,1)} %param.41) | copy-start | bytes 24580
  384.0 66.6 %copy-start.7 = (bf16[4096,8]{0,1:T(8,128)(2,1)S(1)}, bf16[4096,8]{0,1:T(8,128)(2,1)}, u32[]{:S(2)}) copy-start(bf16[4096,8]{0,1:T(8,128)(2,1)} %param.33) | copy-start | bytes 196612
  389.9 86.6 %copy-start.2 = (bf16[32,4096]{1,0:T(8,128)(2,1)S(1)}, bf16[32,4096]{1,0:T(8,128)(2,1)}, u32[]{:S(2)}) copy-start(bf16[32,4096]{1,0:T(8,128)(2,1)} %all-reduce.4.cloned.1.call-done) | copy-start | bytes 786436
  445.3 31.2 %all-to-all-start.3 = ((bf16[8,16,4096]{2,1,0:T(8,128)(2,1)}), bf16[8,16,4096]{2,1,0:T(8,128)(2,1)S(1)}, u32[]{:S(2)}, u32[]{:S(2)}) async-start(bf16[8,16,4096]{2,1,0:T(8,128)(2,1)} %get-tuple-element.3), calls=%async_computation.4 | async-start | bytes 2097152 | tf_op jit(solution)/shard_map/all_to_all | solution.py:126
Sparse Core Ops, SparseCore 0:
  38.8 49.6 reduce-scatter.2
  236.3 41.9 all-reduce.3
  296.1 30.6 reduce-scatter.4
  328.2 49.0 all-gather.1
  390.0 55.1 all-reduce.5
